TPU v7x, 32 devices: a whole 2x2x4 slice. The times are simulated.
32 devices in a mesh: fs: 8 (over z, y), tp: 4 (over x, core).
Axes of the slice: x: 2, y: 2, z: 4, core: 2. Of those that a mesh axis runs over, the one named last changes fastest.
Arguments:
- layer_input: bfloat16 [20480, 4096], P('fs'), may hold values from -140 to 140
- query_cotangent: bfloat16 [20480, 2048], P('fs', 'tp'), may hold values from -0.46817673 to 0.46817673
- value_cotangent: bfloat16 [20480, 512], P('fs', 'tp'), may hold values from -0.46817673 to 0.46817673
- query_weight: float32 [4096, 2048], P('fs', 'tp'), may hold values from -0.09375 to 0.09375
- value_weight: float32 [4096, 512], P('fs', 'tp'), may hold values from -0.09375 to 0.09375
- query_moment: float32 [4096, 2048], P('fs', 'tp'), may hold values from -18 to 18
- value_moment: float32 [4096, 512], P('fs', 'tp'), may hold values from -18 to 18
- query_left_stat: float32 [16, 256, 256], P('fs'), may hold values from -24 to 24
- value_left_stat: float32 [16, 256, 256], P('fs'), may hold values from -24 to 24
- query_right_stat: float32 [32, 64, 64], P('tp'), may hold values from -24 to 24
- value_right_stat: float32 [8, 64, 64], P('tp'), may hold values from -24 to 24
- query_left_root: bfloat16 [16, 256, 256], P('fs'), may hold values from -1.5 to 2
- value_left_root: bfloat16 [16, 256, 256], P('fs'), may hold values from -1.5 to 2
- query_right_root: bfloat16 [32, 64, 64], P('tp'), may hold values from -1.5 to 2
- value_right_root: bfloat16 [8, 64, 64], P('tp'), may hold values from -1.5 to 2
Outputs:
- query_update: float32 [4096, 2048], P('fs', 'tp')
- value_update: float32 [4096, 512], P('fs', 'tp')
- query_moment_new: float32 [4096, 2048], P('fs', 'tp')
- value_moment_new: float32 [4096, 512], P('fs', 'tp')
- query_left_new: float32 [16, 256, 256], P('fs')
- value_left_new: float32 [16, 256, 256], P('fs')
- query_right_new: float32 [32, 64, 64], P('tp')
- value_right_new: float32 [8, 64, 64], P('tp')
- query_copy: bfloat16 [4096, 2048], P(None, 'tp')
- value_copy: bfloat16 [4096, 512], P(None, 'tp')
All inputs are finite; a program needn't handle non-finite values.
Results may differ from a plain program's by a relative error of at most 0.0075.
Values may be sent and summed in bfloat16 or wider, within the bound.
A program may use at most 128 MiB of HBM per device.

v0:
```python
import jax
import jax.numpy as jnp
from jax import lax
from jax.sharding import PartitionSpec as P

D = 4096
HEAD = 64
BLOCK = 256
Q_COLS = 2048
V_COLS = 512
momentum_decay = 0.9
statistic_decay = 0.9
learning_rate = 0.002
epsilon = 1e-06
highest = lax.Precision.HIGHEST


def token_sum(inputs, cotangent):
    return lax.dot_general(
        inputs, cotangent, (((0,), (0,)), ((), ())), preferred_element_type=jnp.float32
    )


def precondition(moment, left_root, right_root):
    shard_rows, columns = moment.shape
    head_count = columns // HEAD
    by_head = jnp.einsum(
        "rhk,hkl->rhl",
        moment.reshape(shard_rows, head_count, HEAD),
        right_root.astype(jnp.float32),
        precision=highest,
    )
    by_block = by_head.reshape(shard_rows // BLOCK, BLOCK, columns)
    return jnp.einsum(
        "bij,bjc->bic", left_root.astype(jnp.float32), by_block, precision=highest
    ).reshape(shard_rows, columns)


def local_terms(gradient, moment, left_root, right_root):
    shard_rows, columns = gradient.shape
    moment_new = momentum_decay * moment + (1.0 - momentum_decay) * gradient
    blocks = gradient.reshape(shard_rows // BLOCK, BLOCK, columns)
    left_part = jnp.einsum("bic,bjc->bij", blocks, blocks, precision=highest)
    per_head = gradient.reshape(shard_rows, columns // HEAD, HEAD)
    right_part = jnp.einsum("rhk,rhl->hkl", per_head, per_head, precision=highest)
    direction = precondition(moment_new, left_root, right_root)
    squares = jnp.stack([jnp.sum(moment_new * moment_new), jnp.sum(direction * direction)])
    return (moment_new, left_part, right_part, direction, squares)


def local(
    layer_input,
    query_cotangent,
    value_cotangent,
    query_weight,
    value_weight,
    query_moment,
    value_moment,
    query_left_stat,
    value_left_stat,
    query_right_stat,
    value_right_stat,
    query_left_root,
    value_left_root,
    query_right_root,
    value_right_root,
):
    query_width = query_cotangent.shape[1]
    both_cotangents = jnp.concatenate([query_cotangent, value_cotangent], axis=1)
    both_gradients = lax.psum_scatter(
        token_sum(layer_input, both_cotangents), "fs", scatter_dimension=0, tiled=True
    )
    query_gradient = both_gradients[:, :query_width]
    value_gradient = both_gradients[:, query_width:]
    query_moment_new, query_left_part, query_right_part, query_direction, query_squares = (
        local_terms(query_gradient, query_moment, query_left_root, query_right_root)
    )
    value_moment_new, value_left_part, value_right_part, value_direction, value_squares = (
        local_terms(value_gradient, value_moment, value_left_root, value_right_root)
    )
    squares = jnp.concatenate([query_squares, value_squares])
    query_right_sum, value_right_sum = (
        lax.psum(query_right_part.astype(jnp.bfloat16), "fs").astype(jnp.float32),
        lax.psum(value_right_part.astype(jnp.bfloat16), "fs").astype(jnp.float32),
    )
    query_left_sum, value_left_sum = (
        lax.psum(query_left_part.astype(jnp.bfloat16), "tp").astype(jnp.float32),
        lax.psum(value_left_part.astype(jnp.bfloat16), "tp").astype(jnp.float32),
    )
    all_squares = lax.psum(squares, ("fs", "tp"))
    query_left_new = (
        statistic_decay * query_left_stat + (1.0 - statistic_decay) / Q_COLS * query_left_sum
    )
    value_left_new = (
        statistic_decay * value_left_stat + (1.0 - statistic_decay) / V_COLS * value_left_sum
    )
    query_right_new = (
        statistic_decay * query_right_stat + (1.0 - statistic_decay) / D * query_right_sum
    )
    value_right_new = (
        statistic_decay * value_right_stat + (1.0 - statistic_decay) / D * value_right_sum
    )
    query_update = jnp.sqrt(all_squares[0] / (all_squares[1] + epsilon)) * query_direction
    value_update = jnp.sqrt(all_squares[2] / (all_squares[3] + epsilon)) * value_direction
    query_shard = (query_weight - learning_rate * query_update).astype(jnp.bfloat16)
    value_shard = (value_weight - learning_rate * value_update).astype(jnp.bfloat16)
    query_copy, value_copy = (
        lax.all_gather(query_shard, "fs", axis=0, tiled=True),
        lax.all_gather(value_shard, "fs", axis=0, tiled=True),
    )
    return (
        query_update,
        value_update,
        query_moment_new,
        value_moment_new,
        query_left_new,
        value_left_new,
        query_right_new,
        value_right_new,
        query_copy,
        value_copy,
    )


def solution(mesh):
    placed = (
        P("fs", None),
        P("fs", "tp"),
        P("fs", "tp"),
        P("fs", "tp"),
        P("fs", "tp"),
        P("fs", "tp"),
        P("fs", "tp"),
        P("fs", None, None),
        P("fs", None, None),
        P("tp", None, None),
        P("tp", None, None),
        P("fs", None, None),
        P("fs", None, None),
        P("tp", None, None),
        P("tp", None, None),
    )
    return jax.shard_map(
        local,
        mesh=mesh,
        in_specs=placed,
        out_specs=(
            P("fs", "tp"),
            P("fs", "tp"),
            P("fs", "tp"),
            P("fs", "tp"),
            P("fs", None, None),
            P("fs", None, None),
            P("tp", None, None),
            P("tp", None, None),
            P(None, "tp"),
            P(None, "tp"),
        ),
        check_vma=False,
    )
```

profile of v0, /device:TPU:0, one launch (start us, length us, event | category | flops | bytes accessed | tf_op | source)
XLA Modules:
  0.0 512.9 jit_solution(3195955658530197964)
XLA Ops:
  7.2 21.4 %convolution_bitcast_fusion = f32[4096,640]{0,1:T(8,128)} fusion(bf16[2560,4096]{1,0:T(8,128)(2,1)} %param.15, bf16[2560,128]{1,0:T(8,128)(2,1)} %param.17, bf16[2560,512]{1,0:T(8,128)(2,1)} %param.16), kind=kOutput, calls=%fused_computation | convolution fusion | flops 13428326400 | bytes 34734080 | tf_op jit(solution)/shard_map/dot_general | solution.py:19
  31.0 179.1 %reduce-scatter.2.cloned.1.call-done = f32[512,640]{0,1:T(8,128)} async-done(((f32[4096,640]{0,1:T(8,128)}), f32[512,640]{0,1:T(8,128)}) %reduce-scatter.2.cloned.1.call-update) | async-done | bytes 1310736 | tf_op jit(solution)/shard_map/reduce_scatter | solution.py:70
  210.1 2.2 multiply_reduce_fusion.1
  213.9 1.9 reshape.59
  215.8 2.4 multiply_reduce_fusion.3
  218.9 1.8 convolution_bitcast_fusion.2
  220.7 1.8 reshape.61
  222.5 2.3 multiply_reduce_fusion
  224.8 2.7 multiply_reduce_fusion.2
  227.5 2.7 pad_maximum_fusion
  230.2 39.4 %psum.35 = f32[4]{0:T(128)S(1)} all-reduce(f32[4]{0:T(128)S(1)} %pad_maximum_fusion), channel_id=1, replica_groups=mesh['fs'=8,'tp'=4] {'fs','tp'}, use_global_device_ids=true, to_apply=%region_5.0 | all-reduce | flops 4 | bytes 32 | tf_op jit(solution)/shard_map/psum | solution.py:90
  270.0 1.9 convolution_convert_fusion
  271.8 1.9 copy.53
  273.7 2.3 convolution_convert_fusion.1
  284.3 2.6 subtract_convert_fusion
  288.2 1.8 copy.49
  291.4 36.9 %psum.39 = bf16[2,64,64]{2,1,0:T(8,128)(2,1)S(1)} all-reduce(bf16[2,64,64]{2,1,0:T(8,128)(2,1)S(1)} %convolution_convert_fusion.3), channel_id=1, replica_groups=mesh['fs'=8,'tp'=4] {'fs'}, use_global_device_ids=true, to_apply=%region_9.0 | all-reduce | flops 8192 | bytes 32768 | tf_op jit(solution)/shard_map/psum | solution.py:84
  329.0 19.2 %all-reduce.4.cloned.1.call-done = bf16[8,64,64]{2,1,0:T(8,128)(2,1)} async-done(((bf16[8,64,64]{2,1,0:T(8,128)(2,1)}), bf16[8,64,64]{2,1,0:T(8,128)(2,1)}) %all-reduce.4.cloned.1.call-update) | async-done | bytes 65552 | tf_op jit(solution)/shard_map/psum | solution.py:83
  348.1 1.8 multiply_add_fusion.3
  349.9 34.4 %all-reduce.6.cloned.1.call-done = (bf16[2,256,256]{2,1,0:T(8,128)(2,1)}, bf16[2,256,256]{2,1,0:T(8,128)(2,1)}) async-done(((bf16[2,256,256]{2,1,0:T(8,128)(2,1)}, bf16[2,256,256]{2,1,0:T(8,128)(2,1)}), (bf16[2,256,256]{2,1,0:T(8,128)(2,1)}, bf16[2,256,256]{2,1,0:T(8,128)(2,1)})) %all-reduce.6.cloned.1.call-update) | async-done | bytes 524304 | tf_op jit(solution)/shard_map/psum | solution.py:87
  384.3 2.2 multiply_add_fusion.1
  386.5 40.3 %all-gather.5.cloned.1.call-done = bf16[4096,128]{1,0:T(8,128)(2,1)} async-done(((bf16[512,128]{1,0:T(8,128)(2,1)}), bf16[4096,128]{1,0:T(8,128)(2,1)}) %all-gather.5.cloned.1.call-update) | async-done | bytes 1048592 | tf_op jit(solution)/shard_map/all_gather | solution.py:109
  426.7 74.1 %all-gather.3.cloned.1.call-done = bf16[4096,512]{1,0:T(8,128)(2,1)} async-done(((bf16[512,512]{1,0:T(8,128)(2,1)}), bf16[4096,512]{1,0:T(8,128)(2,1)}) %all-gather.3.cloned.1.call-update) | async-done | bytes 4194320 | tf_op jit(solution)/shard_map/all_gather | solution.py:108
  500.8 4.6 copy.67
  (48 shorter events, 14.9 us)
Async XLA Ops:
  7.2 215.3 %copy-start = (bf16[2,256,256]{2,1,0:T(8,128)(2,1)S(1)}, bf16[2,256,256]{2,1,0:T(8,128)(2,1)}, u32[]{:S(2)}) copy-start(bf16[2,256,256]{2,1,0:T(8,128)(2,1)} %param.26) | copy-start | bytes 786436
  7.2 202.9 %reduce-scatter.2.cloned.1.call-start = ((), (), s32[]{:S(2)}) async-start(), calls=%async_computation.1 | async-start | bytes 11796480 | tf_op jit(solution)/shard_map/reduce_scatter | solution.py:70
  28.6 1.2 copy-start.4
  28.6 1.6 copy-start.9
  28.6 183.7 %copy-start.10 = (bf16[8,64,64]{2,1,0:T(8,128)(2,1)S(1)}, bf16[8,64,64]{2,1,0:T(8,128)(2,1)}, u32[]{:S(2)}) copy-start(bf16[8,64,64]{2,1,0:T(8,128)(2,1)} %param.28) | copy-start | bytes 196612
  28.6 319.5 %all-reduce.4.cloned.1.call-start = ((), (), s32[]{:S(2)}) async-start(), calls=%async_computation.2 | async-start | bytes 262144 | tf_op jit(solution)/shard_map/psum | solution.py:83
  218.2 0.7 copy-start.3
  271.8 12.3 %copy-start.1 = (f32[2,512,256]{1,2,0:T(8,128)S(1)}, f32[2,512,256]{1,2,0:T(8,128)}, u32[]{:S(2)}) copy-start(f32[2,512,256]{1,2,0:T(8,128)} %get-tuple-element.45) | copy-start | bytes 3145732
  277.8 106.6 %all-reduce.6.cloned.1.call-start = ((), (), s32[]{:S(2)}) async-start(), calls=%async_computation.5 | async-start | bytes 1048576 | tf_op jit(solution)/shard_map/psum | solution.py:87
  279.8 147.0 %all-gather.5.cloned.1.call-start = ((), (), s32[]{:S(2)}) async-start(), calls=%async_computation.4 | async-start | bytes 1179648 | tf_op jit(solution)/shard_map/all_gather | solution.py:109
  280.9 3.2 copy-start.6
  282.7 218.1 %all-gather.3.cloned.1.call-start = ((), (), s32[]{:S(2)}) async-start(), calls=%async_computation.3 | async-start | bytes 4718592 | tf_op jit(solution)/shard_map/all_gather | solution.py:108
  284.1 44.2 %copy-start.11 = (f32[2,64,64]{2,1,0:T(8,128)S(1)}, f32[2,64,64]{2,1,0:T(8,128)}, u32[]{:S(2)}) copy-start(f32[2,64,64]{2,1,0:T(8,128)} %param.25) | copy-start | bytes 98308
  284.2 102.3 %copy-start.2 = (f32[2,512,256]{1,2,0:T(8,128)}, f32[2,512,256]{1,2,0:T(8,128)S(1)}, u32[]{:S(2)}) copy-start(f32[2,512,256]{1,2,0:T(8,128)S(1)} %broadcast_multiply_fusion) | copy-start | bytes 3145732
  284.2 100.1 %copy-start.7 = (f32[2,256,256]{2,1,0:T(8,128)S(1)}, f32[2,256,256]{2,1,0:T(8,128)}, u32[]{:S(2)}) copy-start(f32[2,256,256]{2,1,0:T(8,128)} %param.23) | copy-start | bytes 1572868
  284.2 100.1 %copy-start.8 = (f32[2,256,256]{2,1,0:T(8,128)S(1)}, f32[2,256,256]{2,1,0:T(8,128)}, u32[]{:S(2)}) copy-start(f32[2,256,256]{2,1,0:T(8,128)} %param.22) | copy-start | bytes 1572868
  500.8 4.6 copy-start.5
Sparse Core Ops, SparseCore 0:
  28.8 181.3 reduce-scatter.1
  277.9 70.1 all-reduce.3
  351.7 32.5 all-reduce.5
  386.3 40.3 all-gather.4
  429.3 71.4 all-gather.2
where the time goes:
time: 514 us; the launch traced here: 513 us
  waiting for transfers between devices  347 us (68%)
  blocking collectives  76.3 us (15%)
  matrix products  37.1 us (7%)
  local copies, waits for them, and re-layouts  18.3 us (4%)
  other arithmetic  17.2 us (3%)
  between operations  16.6 us (3%)
    reduce_scatter x1, waiting for transfers between devices, local(): lax.psum_scatter(token_sum(layer_input, both_cotangents), 'fs', scatter_d...  179 us
    all_gather x1, waiting for transfers between devices, local(): lax.all_gather(query_shard, 'fs', axis=0, tiled=True)  74.1 us
    all_gather x1, waiting for transfers between devices, local(): lax.all_gather(value_shard, 'fs', axis=0, tiled=True)  40.3 us
    psum x1, blocking collectives, local(): all_squares = lax.psum(squares, ('fs', 'tp'))  39.4 us
    psum x1, blocking collectives, local(): lax.psum(value_right_part.astype(jnp.bfloat16), 'fs').astype(jnp.float32)  36.9 us
    psum x1, waiting for transfers between devices, local(): lax.psum(query_left_part.astype(jnp.bfloat16), 'tp').astype(jnp.float32)  34.4 us
    dot_general x1, matrix products, token_sum(): lax.dot_general(inputs, cotangent, (((0,), (0,)), ((), ())), preferred_el...  21.4 us
    psum x1, waiting for transfers between devices, local(): lax.psum(query_right_part.astype(jnp.bfloat16), 'fs').astype(jnp.float32)  19.2 us
  transfers between devices with their start and end apart: 5, of which 5 were waited for; matrix products, arithmetic and copies ran while one was open for 3% of the time, Pallas kernels for 0%

commit v1 on v0

--- a/solution.py
+++ b/solution.py
@@ -87,7 +87,7 @@
         lax.psum(query_left_part.astype(jnp.bfloat16), "tp").astype(jnp.float32),
         lax.psum(value_left_part.astype(jnp.bfloat16), "tp").astype(jnp.float32),
     )
-    all_squares = lax.psum(squares, ("fs", "tp"))
+    all_squares = lax.psum(lax.psum(squares, "tp"), "fs")
     query_left_new = (
         statistic_decay * query_left_stat + (1.0 - statistic_decay) / Q_COLS * query_left_sum
     )

time: 514 us -> 497 us (0.967)
  blocking collectives: 76.3 us -> 59.5 us
    psum x1 -> x2, blocking collectives: 39.4 us -> 26.4 us  [local(): all_squares = lax.psum(lax.psum(squares, 'tp'), 'fs')]
where the time goes in v1:
time: 497 us; the launch traced here: 496 us
  waiting for transfers between devices  347 us (70%)
  blocking collectives  59.5 us (12%)
  matrix products  37.1 us (7%)
  local copies, waits for them, and re-layouts  18.3 us (4%)
  other arithmetic  17.2 us (3%)
  between operations  16.6 us (3%)
    reduce_scatter x1, waiting for transfers between devices, local(): lax.psum_scatter(token_sum(layer_input, both_cotangents), 'fs', scatter_d...  179 us
    all_gather x1, waiting for transfers between devices, local(): lax.all_gather(query_shard, 'fs', axis=0, tiled=True)  74.1 us
    all_gather x1, waiting for transfers between devices, local(): lax.all_gather(value_shard, 'fs', axis=0, tiled=True)  40.3 us
    psum x1, waiting for transfers between devices, local(): lax.psum(query_left_part.astype(jnp.bfloat16), 'tp').astype(jnp.float32)  34.4 us
    psum x1, blocking collectives, local(): lax.psum(value_right_part.astype(jnp.bfloat16), 'fs').astype(jnp.float32)  33 us
    psum x2, blocking collectives, local(): all_squares = lax.psum(lax.psum(squares, 'tp'), 'fs')  26.4 us
    dot_general x1, matrix products, token_sum(): lax.dot_general(inputs, cotangent, (((0,), (0,)), ((), ())), preferred_el...  21.3 us
    psum x1, waiting for transfers between devices, local(): lax.psum(query_right_part.astype(jnp.bfloat16), 'fs').astype(jnp.float32)  19.5 us
  transfers between devices with their start and end apart: 5, of which 5 were waited for; matrix products, arithmetic and copies ran while one was open for 3% of the time, Pallas kernels for 0%

profile of v1, /device:TPU:0, one launch (start us, length us, event | category | flops | bytes accessed | tf_op | source)
XLA Modules:
  0.0 496.3 jit_solution(1870781038408484861)
XLA Ops:
  7.2 21.3 %convolution_bitcast_fusion = f32[4096,640]{0,1:T(8,128)} fusion(bf16[2560,4096]{1,0:T(8,128)(2,1)} %param.15, bf16[2560,128]{1,0:T(8,128)(2,1)} %param.17, bf16[2560,512]{1,0:T(8,128)(2,1)} %param.16), kind=kOutput, calls=%fused_computation | convolution fusion | flops 13428326400 | bytes 34734080 | tf_op jit(solution)/shard_map/dot_general | solution.py:19
  30.9 179.1 %reduce-scatter.2.cloned.1.call-done = f32[512,640]{0,1:T(8,128)} async-done(((f32[4096,640]{0,1:T(8,128)}), f32[512,640]{0,1:T(8,128)}) %reduce-scatter.2.cloned.1.call-update) | async-done | bytes 1310736 | tf_op jit(solution)/shard_map/reduce_scatter | solution.py:70
  210.1 2.2 multiply_reduce_fusion.1
  213.9 1.9 reshape.59
  215.8 2.4 multiply_reduce_fusion.3
  218.8 1.8 convolution_bitcast_fusion.2
  220.6 1.8 reshape.61
  222.4 2.3 multiply_reduce_fusion
  224.7 2.7 multiply_reduce_fusion.2
  227.4 2.7 pad_maximum_fusion
  230.1 6.5 %psum.42 = f32[4]{0:T(128)S(1)} all-reduce(f32[4]{0:T(128)S(1)} %pad_maximum_fusion), channel_id=1, replica_groups=mesh['fs'=8,'tp'=4] {'tp'}, use_global_device_ids=true, to_apply=%region_5.0 | all-reduce | flops 4 | bytes 32 | tf_op jit(solution)/shard_map/psum | solution.py:90
  236.6 20.0 %psum.43 = f32[4]{0:T(128)S(1)} all-reduce(f32[4]{0:T(128)S(1)} %psum.42), channel_id=1, replica_groups=mesh['fs'=8,'tp'=4] {'fs'}, use_global_device_ids=true, to_apply=%region_6.0 | all-reduce | flops 4 | bytes 32 | tf_op jit(solution)/shard_map/psum | solution.py:90
  256.9 1.9 convolution_convert_fusion
  258.7 1.9 copy.53
  260.6 2.3 convolution_convert_fusion.1
  271.2 2.6 subtract_convert_fusion
  275.1 1.8 copy.49
  278.3 33.0 %psum.47 = bf16[2,64,64]{2,1,0:T(8,128)(2,1)S(1)} all-reduce(bf16[2,64,64]{2,1,0:T(8,128)(2,1)S(1)} %convolution_convert_fusion.3), channel_id=1, replica_groups=mesh['fs'=8,'tp'=4] {'fs'}, use_global_device_ids=true, to_apply=%region_10.0 | all-reduce | flops 8192 | bytes 32768 | tf_op jit(solution)/shard_map/psum | solution.py:84
  312.0 19.5 %all-reduce.4.cloned.1.call-done = bf16[8,64,64]{2,1,0:T(8,128)(2,1)} async-done(((bf16[8,64,64]{2,1,0:T(8,128)(2,1)}), bf16[8,64,64]{2,1,0:T(8,128)(2,1)}) %all-reduce.4.cloned.1.call-update) | async-done | bytes 65552 | tf_op jit(solution)/shard_map/psum | solution.py:83
  333.3 34.4 %all-reduce.6.cloned.1.call-done = (bf16[2,256,256]{2,1,0:T(8,128)(2,1)}, bf16[2,256,256]{2,1,0:T(8,128)(2,1)}) async-done(((bf16[2,256,256]{2,1,0:T(8,128)(2,1)}, bf16[2,256,256]{2,1,0:T(8,128)(2,1)}), (bf16[2,256,256]{2,1,0:T(8,128)(2,1)}, bf16[2,256,256]{2,1,0:T(8,128)(2,1)})) %all-reduce.6.cloned.1.call-update) | async-done | bytes 524304 | tf_op jit(solution)/shard_map/psum | solution.py:87
  367.8 2.2 multiply_add_fusion.1
  369.9 40.3 %all-gather.5.cloned.1.call-done = bf16[4096,128]{1,0:T(8,128)(2,1)} async-done(((bf16[512,128]{1,0:T(8,128)(2,1)}), bf16[4096,128]{1,0:T(8,128)(2,1)}) %all-gather.5.cloned.1.call-update) | async-done | bytes 1048592 | tf_op jit(solution)/shard_map/all_gather | solution.py:109
  410.2 74.1 %all-gather.3.cloned.1.call-done = bf16[4096,512]{1,0:T(8,128)(2,1)} async-done(((bf16[512,512]{1,0:T(8,128)(2,1)}), bf16[4096,512]{1,0:T(8,128)(2,1)}) %all-gather.3.cloned.1.call-update) | async-done | bytes 4194320 | tf_op jit(solution)/shard_map/all_gather | solution.py:108
  484.3 4.6 copy.67
  (49 shorter events, 16.7 us)
Async XLA Ops:
  7.2 215.3 %copy-start = (bf16[2,256,256]{2,1,0:T(8,128)(2,1)S(1)}, bf16[2,256,256]{2,1,0:T(8,128)(2,1)}, u32[]{:S(2)}) copy-start(bf16[2,256,256]{2,1,0:T(8,128)(2,1)} %param.26) | copy-start | bytes 786436
  7.2 202.9 %reduce-scatter.2.cloned.1.call-start = ((), (), s32[]{:S(2)}) async-start(), calls=%async_computation.1 | async-start | bytes 11796480 | tf_op jit(solution)/shard_map/reduce_scatter | solution.py:70
  28.5 1.2 copy-start.4
  28.5 1.6 copy-start.9
  28.6 183.7 %copy-start.10 = (bf16[8,64,64]{2,1,0:T(8,128)(2,1)S(1)}, bf16[8,64,64]{2,1,0:T(8,128)(2,1)}, u32[]{:S(2)}) copy-start(bf16[8,64,64]{2,1,0:T(8,128)(2,1)} %param.28) | copy-start | bytes 196612
  28.6 303.0 %all-reduce.4.cloned.1.call-start = ((), (), s32[]{:S(2)}) async-start(), calls=%async_computation.2 | async-start | bytes 262144 | tf_op jit(solution)/shard_map/psum | solution.py:83
  218.1 0.7 copy-start.3
  258.7 12.3 %copy-start.1 = (f32[2,512,256]{1,2,0:T(8,128)S(1)}, f32[2,512,256]{1,2,0:T(8,128)}, u32[]{:S(2)}) copy-start(f32[2,512,256]{1,2,0:T(8,128)} %get-tuple-element.45) | copy-start | bytes 3145732
  264.7 103.1 %all-reduce.6.cloned.1.call-start = ((), (), s32[]{:S(2)}) async-start(), calls=%async_computation.5 | async-start | bytes 1048576 | tf_op jit(solution)/shard_map/psum | solution.py:87
  266.7 143.5 %all-gather.5.cloned.1.call-start = ((), (), s32[]{:S(2)}) async-start(), calls=%async_computation.4 | async-start | bytes 1179648 | tf_op jit(solution)/shard_map/all_gather | solution.py:109
  267.9 3.2 copy-start.6
  269.6 214.6 %all-gather.3.cloned.1.call-start = ((), (), s32[]{:S(2)}) async-start(), calls=%async_computation.3 | async-start | bytes 4718592 | tf_op jit(solution)/shard_map/all_gather | solution.py:108
  271.0 40.3 %copy-start.11 = (f32[2,64,64]{2,1,0:T(8,128)S(1)}, f32[2,64,64]{2,1,0:T(8,128)}, u32[]{:S(2)}) copy-start(f32[2,64,64]{2,1,0:T(8,128)} %param.25) | copy-start | bytes 98308
  271.1 98.8 %copy-start.2 = (f32[2,512,256]{1,2,0:T(8,128)}, f32[2,512,256]{1,2,0:T(8,128)S(1)}, u32[]{:S(2)}) copy-start(f32[2,512,256]{1,2,0:T(8,128)S(1)} %broadcast_multiply_fusion) | copy-start | bytes 3145732
  271.2 96.6 %copy-start.7 = (f32[2,256,256]{2,1,0:T(8,128)S(1)}, f32[2,256,256]{2,1,0:T(8,128)}, u32[]{:S(2)}) copy-start(f32[2,256,256]{2,1,0:T(8,128)} %param.23) | copy-start | bytes 1572868
  271.2 96.6 %copy-start.8 = (f32[2,256,256]{2,1,0:T(8,128)S(1)}, f32[2,256,256]{2,1,0:T(8,128)}, u32[]{:S(2)}) copy-start(f32[2,256,256]{2,1,0:T(8,128)} %param.22) | copy-start | bytes 1572868
  484.2 4.6 copy-start.5
Sparse Core Ops, SparseCore 0:
  28.7 181.3 reduce-scatter.1
  264.8 66.6 all-reduce.3
  335.1 32.5 all-reduce.5
  369.7 40.3 all-gather.4
  412.7 71.4 all-gather.2
